TPU v7x, 32 devices: a whole 2x2x4 slice. The times are simulated.
32 devices in a mesh: ep: 16 (over z, y, x), tp: 2 (over core).
Axes of the slice: x: 2, y: 2, z: 4, core: 2. Of those that a mesh axis runs over, the one named last changes fastest.
Arguments:
- tokens: bfloat16 [512, 2048], P('ep'), may hold values from -6 to 6
- mix_gain: float32 [2048], replicated, may hold values from 0.1 to 1.9
- w_query: bfloat16 [2048, 512], P('ep', 'tp'), may hold values from -0.125 to 0.125
- w_key: bfloat16 [2048, 512], P('ep', 'tp'), may hold values from -0.125 to 0.125
- w_value: bfloat16 [2048, 512], P('ep', 'tp'), may hold values from -0.125 to 0.125
- w_outgate: bfloat16 [2048, 512], P('ep', 'tp'), may hold values from -0.125 to 0.125
- w_igate: bfloat16 [2048, 8], P('ep', 'tp'), may hold values from -0.125 to 0.125
- w_fgate: bfloat16 [2048, 8], P('ep', 'tp'), may hold values from -0.125 to 0.125
- igate_bias: float32 [8], P('tp'), may hold values from -2 to 1
- fgate_bias: float32 [8], P('tp'), may hold values from 0 to 4
- head_gain: float32 [512], P('tp'), may hold values from 0.1 to 1.9
- w_out: bfloat16 [512, 2048], P('tp', 'ep'), may hold values from -0.25 to 0.25
- state_matrix: float32 [512, 8, 64, 64], P('ep', 'tp'), may hold values from -2.4 to 2.4
- state_norm: float32 [512, 8, 64], P('ep', 'tp'), may hold values from -2.4 to 2.4
- state_max: float32 [512, 8], P('ep', 'tp'), may hold values from -4 to 4
- ffn_gain: float32 [2048], replicated, may hold values from 0.1 to 1.9
- w_expert_gate: bfloat16 [16, 2048, 1408], P('ep', None, 'tp'), may hold values from -0.125 to 0.125
- w_expert_up: bfloat16 [16, 2048, 1408], P('ep', None, 'tp'), may hold values from -0.125 to 0.125
- w_expert_down: bfloat16 [16, 1408, 2048], P('ep', 'tp'), may hold values from -0.15625 to 0.15625
- routes: int32 [512, 3], P('ep'), may hold values from 0 to 15, all different within a row; in each aligned block of 32 rows (0 to 31, 32 to 63, ...) at most 12 rows name the same one
- route_weights: float32 [512, 3], P('ep'), may hold values from 0.2 to 1
Outputs:
- mixed: bfloat16 [512, 2048], P('ep')
- new_matrix: float32 [512, 8, 64, 64], P('ep', 'tp')
- new_norm: float32 [512, 8, 64], P('ep', 'tp')
- new_max: float32 [512, 8], P('ep', 'tp')
Inputs may be any that keep to these rules, and one draw needn't show every extreme that they name: `routes`: each row names 3 different experts. Among the rows of one device, no expert is named by more than 12 rows, a bound that some block reaches.
All inputs are finite; a program needn't handle non-finite values.
Results may differ from a plain program's by a relative error of at most 0.017.
Values may be sent and summed in bfloat16 or wider, within the bound.
A program may use at most 128 MiB of HBM per device.

v0:
```python
import jax
import jax.numpy as jnp
from jax import lax
from jax.sharding import PartitionSpec as P


def rms_scale(values_in, gain_vec):
    widened = values_in.astype(jnp.float32)
    return (
        widened * lax.rsqrt(jnp.mean(widened * widened, axis=-1, keepdims=True) + 1e-06) * gain_vec
    )


def memory_cell(
    query,
    key_row,
    value_row,
    outgate,
    input_pre,
    forget_pre,
    head_gain,
    state_matrix,
    state_norm,
    state_max,
):
    seq_rows, head_count = input_pre.shape
    head_size = query.shape[1] // head_count
    query_heads = query.astype(jnp.float32).reshape(seq_rows, head_count, head_size)
    key_heads = key_row.astype(jnp.float32).reshape(
        seq_rows, head_count, head_size
    ) * head_size ** (-0.5)
    value_heads = value_row.astype(jnp.float32).reshape(seq_rows, head_count, head_size)
    log_forget = jax.nn.log_sigmoid(forget_pre)
    new_max = jnp.maximum(log_forget + state_max, input_pre)
    keep_old = jnp.exp(log_forget + state_max - new_max)
    keep_new = jnp.exp(input_pre - new_max)
    new_matrix = (
        keep_old[:, :, None, None] * state_matrix
        + keep_new[:, :, None, None] * value_heads[:, :, :, None] * key_heads[:, :, None, :]
    )
    new_norm = keep_old[:, :, None] * state_norm + keep_new[:, :, None] * key_heads
    numerator = jnp.einsum(
        "bhvd,bhd->bhv", new_matrix, query_heads, precision=lax.Precision.HIGHEST
    )
    denominator = jnp.sum(new_norm * query_heads, axis=-1)
    cell_read = numerator / jnp.maximum(jnp.abs(denominator), jnp.exp(-new_max))[:, :, None]
    centered = cell_read - jnp.mean(cell_read, axis=-1, keepdims=True)
    variance = jnp.mean(centered * centered, axis=-1, keepdims=True)
    scaled_cell = (centered * lax.rsqrt(variance + 1e-06)).reshape(seq_rows, head_count * head_size)
    cell_out = (scaled_cell * head_gain * jax.nn.sigmoid(outgate.astype(jnp.float32))).astype(
        jnp.bfloat16
    )
    return (cell_out, new_matrix, new_norm, new_max)


def body(
    tokens,
    mix_gain,
    w_query,
    w_key,
    w_value,
    w_outgate,
    w_igate,
    w_fgate,
    igate_bias,
    fgate_bias,
    head_gain,
    w_out,
    state_matrix,
    state_norm,
    state_max,
    ffn_gain,
    w_expert_gate,
    w_expert_up,
    w_expert_down,
    routes,
    route_weights,
):
    seq_rows, width = tokens.shape
    normed = rms_scale(tokens, mix_gain).astype(jnp.bfloat16)
    weight_list = (w_query, w_key, w_value, w_outgate, w_igate, w_fgate)
    spread = lax.all_to_all(normed, "ep", split_axis=1, concat_axis=0, tiled=True)
    joined = jnp.concatenate(weight_list, axis=1)
    summed = lax.psum_scatter(
        jnp.dot(spread, joined, preferred_element_type=jnp.float32),
        "ep",
        scatter_dimension=0,
        tiled=True,
    )
    bounds = [0]
    for weight in weight_list:
        bounds.append(bounds[-1] + weight.shape[1])
    projected = tuple(
        (summed[:, bounds[index] : bounds[index + 1]] for index in range(len(weight_list)))
    )
    query = projected[0].astype(jnp.bfloat16)
    key_row = projected[1].astype(jnp.bfloat16)
    value_row = projected[2].astype(jnp.bfloat16)
    outgate = projected[3].astype(jnp.bfloat16)
    input_pre = projected[4] + igate_bias
    forget_pre = projected[5] + fgate_bias
    cell_out, new_matrix, new_norm, new_max = memory_cell(
        query,
        key_row,
        value_row,
        outgate,
        input_pre,
        forget_pre,
        head_gain,
        state_matrix,
        state_norm,
        state_max,
    )
    partial_out = jnp.dot(
        cell_out,
        lax.all_gather(w_out, "ep", axis=1, tiled=True),
        preferred_element_type=jnp.float32,
    )
    attended = lax.psum(partial_out.astype(jnp.bfloat16), "tp").astype(jnp.float32)
    resid = (tokens.astype(jnp.float32) + attended).astype(jnp.bfloat16)
    normed_two = rms_scale(resid, ffn_gain).astype(jnp.bfloat16)
    ep_count = lax.axis_size("ep")
    local_experts = w_expert_gate.shape[0]
    expert_total = local_experts * ep_count
    top_count = routes.shape[1]
    capacity = max(2, 2 * seq_rows * top_count // expert_total)
    flat_routes = routes.reshape(-1)
    onehot = (flat_routes[:, None] == jnp.arange(expert_total, dtype=jnp.int32)[None, :]).astype(
        jnp.int32
    )
    earlier = jnp.cumsum(onehot, axis=0, dtype=jnp.int32) - onehot
    slots = jnp.sum(onehot * earlier, axis=1, dtype=jnp.int32)
    targets = flat_routes * capacity + slots
    dispatch = (
        targets[:, None] == jnp.arange(expert_total * capacity, dtype=jnp.int32)[None, :]
    ).astype(jnp.bfloat16)
    route_rows = jnp.repeat(normed_two, top_count, axis=0)
    outgoing = jnp.einsum(
        "rs,rd->sd", dispatch, route_rows, preferred_element_type=jnp.float32
    ).astype(jnp.bfloat16)
    outgoing = outgoing.reshape(expert_total, capacity, width)
    received = lax.all_to_all(outgoing, "ep", split_axis=0, concat_axis=0, tiled=True)
    slot_count = received.shape[1]
    regrouped = received.reshape(ep_count, local_experts, slot_count, width)
    gate_pre = jnp.einsum(
        "nxcd,xdf->nxcf", regrouped, w_expert_gate, preferred_element_type=jnp.float32
    )
    up_pre = jnp.einsum(
        "nxcd,xdf->nxcf", regrouped, w_expert_up, preferred_element_type=jnp.float32
    )
    hidden = (jax.nn.silu(gate_pre) * up_pre).astype(jnp.bfloat16)
    partial_down = jnp.einsum(
        "nxcf,xfd->nxcd", hidden, w_expert_down, preferred_element_type=jnp.float32
    )
    expert_sum = lax.psum(partial_down.astype(jnp.bfloat16), "tp")
    finished = expert_sum.reshape(ep_count * local_experts, slot_count, width)
    returned = lax.all_to_all(finished, "ep", split_axis=0, concat_axis=0, tiled=True)
    picked = jnp.dot(
        dispatch,
        returned.reshape(expert_total * capacity, width),
        preferred_element_type=jnp.float32,
    )
    weighted = jnp.sum(
        picked.reshape(seq_rows, top_count, width) * route_weights[:, :, None], axis=1
    )
    mixed = (resid.astype(jnp.float32) + weighted).astype(jnp.bfloat16)
    return (mixed, new_matrix, new_norm, new_max)


def solution(mesh):
    placed = (
        P("ep", None),
        P(),
        P("ep", "tp"),
        P("ep", "tp"),
        P("ep", "tp"),
        P("ep", "tp"),
        P("ep", "tp"),
        P("ep", "tp"),
        P("tp"),
        P("tp"),
        P("tp"),
        P("tp", "ep"),
        P("ep", "tp", None, None),
        P("ep", "tp", None),
        P("ep", "tp"),
        P(),
        P("ep", None, "tp"),
        P("ep", None, "tp"),
        P("ep", "tp", None),
        P("ep", None),
        P("ep", None),
    )
    return jax.shard_map(
        body,
        mesh=mesh,
        in_specs=placed,
        out_specs=(P("ep", None), P("ep", "tp", None, None), P("ep", "tp", None), P("ep", "tp")),
        check_vma=False,
    )
```

profile of v0, /device:TPU:29, one launch (start us, length us, event | category | flops | bytes accessed | tf_op | source)
XLA Modules:
  0.0 339.8 jit_solution(8380659892496630698)
XLA Ops:
  7.2 1.2 fusion.36
  8.4 1.7 copy_bitcast_fusion
  10.1 6.4 %all-to-all-start = ((bf16[32,16,128]{2,0,1:T(8,128)(2,1)}), bf16[32,16,128]{2,0,1:T(8,128)(2,1)S(1)}, u32[]{:S(2)}, u32[]{:S(2)}) async-start(bf16[32,16,128]{2,0,1:T(8,128)(2,1)} %copy_bitcast_fusion), calls=%async_computation | async-start | bytes 262144 | tf_op jit(solution)/shard_map/all_to_all | solution.py:82
  20.2 1.9 fusion.62
  23.6 126.8 %reduce-scatter.2.cloned.1.call-done = f32[32,1032]{1,0:T(8,128)} async-done(((f32[512,1032]{1,0:T(8,128)}), f32[32,1032]{1,0:T(8,128)}) %reduce-scatter.2.cloned.1.call-update) | async-done | bytes 132112 | tf_op jit(solution)/shard_map/reduce_scatter | solution.py:84
  154.3 3.8 %multiply_add_fusion = f32[32,4,64,64]{3,2,1,0:T(8,128)S(1)} fusion(f32[32,4,64,64]{3,2,1,0:T(8,128)} %param.33, f32[32,4,64]{2,1,0:T(4,128)S(1)} %get-tuple-element.30, f32[32,4,64]{2,1,0:T(4,128)S(1)} %get-tuple-element.31, f32[32,4]{1,0:T(8,128)S(1)} %subtract_exponential_fusion.1), kind=kLoop, calls=%fused_computation | loop fusion | flops 1572864 | bytes 4260352 | tf_op jit(solution)/shard_map/add | solution.py:38
  158.1 2.0 copy-done.1
  160.1 3.4 fusion.63
  164.1 38.4 %all-gather.2.cloned.1.call-done = bf16[256,2048]{1,0:T(8,128)(2,1)} async-done(((bf16[256,128]{1,0:T(8,128)(2,1)}), bf16[256,2048]{1,0:T(8,128)(2,1)}) %all-gather.2.cloned.1.call-update) | async-done | bytes 1048592 | tf_op jit(solution)/shard_map/all_gather | solution.py:116
  202.5 2.2 convolution_convert_fusion.1
  205.3 21.4 %all-reduce.3.cloned.1.call-done = bf16[32,2048]{1,0:T(8,128)(2,1)} async-done(((bf16[32,2048]{1,0:T(8,128)(2,1)}), bf16[32,2048]{1,0:T(8,128)(2,1)}) %all-reduce.3.cloned.1.call-update) | async-done | bytes 131088 | tf_op jit(solution)/shard_map/psum | solution.py:119
  226.7 1.1 fusion.40
  229.0 1.1 reshape.153
  230.1 2.4 convolution_convert_fusion
  232.5 2.1 reshape.154
  234.6 30.4 %all_to_all.29 = bf16[16,12,2048]{2,1,0:T(8,128)(2,1)S(1)} all-to-all(bf16[16,12,2048]{2,1,0:T(8,128)(2,1)} %reshape.154), channel_id=1, replica_groups=mesh['ep'=16,'tp'=2] {'ep'}, dimensions={0} | all-to-all | bytes 1572864 | tf_op jit(solution)/shard_map/all_to_all | solution.py:142
  266.0 3.8 %fusion.9 = f32[16,1,12,704]{3,0,2,1:T(8,128)} fusion(bf16[1,2048,704]{1,2,0:T(8,128)(2,1)} %param.37, bf16[16,12,2048]{2,1,0:T(8,128)(2,1)S(1)} %all_to_all.29), kind=kOutput, calls=%fused_computation.11 | convolution fusion | flops 553648128 | bytes 4210688 | tf_op jit(solution)/shard_map/nxcd,xdf->nxcf/dot_general | solution.py:145
  269.8 5.2 %fusion.6 = bf16[16,12,2048]{2,0,1:T(8,128)(2,1)} fusion(bf16[1,704,2048]{2,1,0:T(8,128)(2,1)S(1)} %copy-done, bf16[1,2048,704]{1,2,0:T(8,128)(2,1)} %param.38, f32[16,1,12,704]{3,0,2,1:T(8,128)} %fusion.9, bf16[16,12,2048]{2,1,0:T(8,128)(2,1)} %copy-done.4), kind=kOutput, calls=%fused_computation.7 | convolution fusion | flops 1108500480 | bytes 7880704 | tf_op jit(solution)/shard_map/nxcf,xfd->nxcd/dot_general | solution.py:152
  275.0 20.7 %all-reduce.5.cloned.1.call-done = bf16[16,12,2048]{2,0,1:T(8,128)(2,1)} async-done(((bf16[16,12,2048]{2,0,1:T(8,128)(2,1)}), bf16[16,12,2048]{2,0,1:T(8,128)(2,1)}) %all-reduce.5.cloned.1.call-update) | async-done | bytes 786448 | tf_op jit(solution)/shard_map/psum | solution.py:155
  295.7 2.6 copy.65
  298.3 6.5 %all-to-all-start.2 = ((bf16[16,12,2048]{2,1,0:T(8,128)(2,1)}), bf16[16,12,2048]{2,1,0:T(8,128)(2,1)}, u32[]{:S(2)}, u32[]{:S(2)}) async-start(bf16[16,12,2048]{2,1,0:T(8,128)(2,1)} %copy.65), calls=%async_computation.3 | async-start | bytes 2097152 | tf_op jit(solution)/shard_map/all_to_all | solution.py:157
  305.6 23.3 %all-to-all-done.2 = bf16[16,12,2048]{2,1,0:T(8,128)(2,1)} async-done(((bf16[16,12,2048]{2,1,0:T(8,128)(2,1)}), bf16[16,12,2048]{2,1,0:T(8,128)(2,1)}, u32[]{:S(2)}, u32[]{:S(2)}) %all-to-all-start.2) | async-done | bytes 786464 | tf_op jit(solution)/shard_map/all_to_all | solution.py:157
  328.9 2.1 reshape.169
  331.1 1.5 fusion.18
  (75 shorter events, 14.0 us)
Async XLA Ops:
  7.2 262.6 %copy-start = (bf16[1,704,2048]{2,1,0:T(8,128)(2,1)S(1)}, bf16[1,704,2048]{2,1,0:T(8,128)(2,1)}, u32[]{:S(2)}) copy-start(bf16[1,704,2048]{2,1,0:T(8,128)(2,1)} %param.39) | copy-start | bytes 8650756
  10.1 10.2 %all-to-all-start = ((bf16[32,16,128]{2,0,1:T(8,128)(2,1)}), bf16[32,16,128]{2,0,1:T(8,128)(2,1)S(1)}, u32[]{:S(2)}, u32[]{:S(2)}) async-start(bf16[32,16,128]{2,0,1:T(8,128)(2,1)} %copy_bitcast_fusion), calls=%async_computation | async-start | bytes 262144 | tf_op jit(solution)/shard_map/all_to_all | solution.py:82
  16.4 134.0 %reduce-scatter.2.cloned.1.call-start = ((), (), s32[]{:S(2)}) async-start(), calls=%async_computation.4 | async-start | bytes 2506752 | tf_op jit(solution)/shard_map/reduce_scatter | solution.py:84
  18.1 4.8 %copy-start.13 = (f32[32,4]{0,1:T(4,128)S(1)}, f32[32,4]{0,1:T(4,128)}, u32[]{:S(2)}) copy-start(f32[32,4]{0,1:T(4,128)} %param.35) | copy-start | bytes 1540
  18.1 4.9 %copy-start.7 = (s32[32,3]{0,1:T(4,128)S(1)}, s32[32,3]{0,1:T(4,128)}, u32[]{:S(2)}) copy-start(s32[32,3]{0,1:T(4,128)} %param.40) | copy-start | bytes 1156
  20.2 131.5 %copy-start.10 = (f32[4]{0:T(128)S(1)}, f32[4]{0:T(128)}, u32[]{:S(2)}) copy-start(f32[4]{0:T(128)} %param.30) | copy-start | bytes 52
  20.2 131.5 %copy-start.15 = (f32[4]{0:T(128)S(1)}, f32[4]{0:T(128)}, u32[]{:S(2)}) copy-start(f32[4]{0:T(128)} %param.29) | copy-start | bytes 52
  20.2 133.3 %copy-start.5 = (f32[32,4,64]{2,1,0:T(4,128)S(1)}, f32[32,4,64]{2,1,0:T(4,128)}, u32[]{:S(2)}) copy-start(f32[32,4,64]{2,1,0:T(4,128)} %param.34) | copy-start | bytes 98308
  22.1 180.4 %all-gather.2.cloned.1.call-start = ((), (), s32[]{:S(2)}) async-start(), calls=%async_computation.5 | async-start | bytes 1114112 | tf_op jit(solution)/shard_map/all_gather | solution.py:116
  22.8 203.9 %all-reduce.3.cloned.1.call-start = ((), (), s32[]{:S(2)}) async-start(), calls=%async_computation.6 | async-start | bytes 262144 | tf_op jit(solution)/shard_map/psum | solution.py:119
  23.6 181.2 %copy-start.11 = (s32[96]{0:T(128)}, s32[96]{0:T(128)S(1)}, u32[]{:S(2)}) copy-start(s32[96]{0:T(128)S(1)} %select_reduce_fusion) | copy-start | bytes 1156
  158.1 2.0 copy-start.1
  160.1 42.5 %copy-start.14 = (f32[256]{0:T(256)S(1)}, f32[256]{0:T(256)}, u32[]{:S(2)}) copy-start(f32[256]{0:T(256)} %param.31) | copy-start | bytes 3076
  160.1 66.6 %copy-start.2 = (bf16[32,2048]{1,0:T(8,128)(2,1)S(1)}, bf16[32,2048]{1,0:T(8,128)(2,1)}, u32[]{:S(2)}) copy-start(bf16[32,2048]{1,0:T(8,128)(2,1)} %param.21) | copy-start | bytes 393220
  160.1 67.7 %copy-start.6 = (f32[2048]{0:T(1024)S(1)}, f32[2048]{0:T(1024)}, u32[]{:S(2)}) copy-start(f32[2048]{0:T(1024)} %param.36) | copy-start | bytes 24580
  204.7 91.0 %all-reduce.5.cloned.1.call-start = ((), (), s32[]{:S(2)}) async-start(), calls=%async_computation.7 | async-start | bytes 1572864 | tf_op jit(solution)/shard_map/psum | solution.py:155
  265.0 1.0 copy-start.4
  275.0 29.8 %copy-start.12 = (s32[96]{0:T(128)S(1)}, s32[96]{0:T(128)}, u32[]{:S(2)}) copy-start(s32[96]{0:T(128)} %copy-done.11) | copy-start | bytes 1156
  275.0 30.0 %copy-start.8 = (s32[32,3]{0,1:T(4,128)S(1)}, s32[32,3]{0,1:T(4,128)}, u32[]{:S(2)}) copy-start(s32[32,3]{0,1:T(4,128)} %param.40) | copy-start | bytes 1156
  275.0 56.1 %copy-start.9 = (f32[32,3]{0,1:T(4,128)S(1)}, f32[32,3]{0,1:T(4,128)}, u32[]{:S(2)}) copy-start(f32[32,3]{0,1:T(4,128)} %param.41) | copy-start | bytes 1156
  298.3 34.3 %copy-start.3 = (bf16[32,2048]{1,0:T(8,128)(2,1)S(1)}, bf16[32,2048]{1,0:T(8,128)(2,1)}, u32[]{:S(2)}) copy-start(bf16[32,2048]{1,0:T(8,128)(2,1)} %all-reduce.3.cloned.1.call-done) | copy-start | bytes 393220
  298.3 30.7 %all-to-all-start.2 = ((bf16[16,12,2048]{2,1,0:T(8,128)(2,1)}), bf16[16,12,2048]{2,1,0:T(8,128)(2,1)}, u32[]{:S(2)}, u32[]{:S(2)}) async-start(bf16[16,12,2048]{2,1,0:T(8,128)(2,1)} %copy.65), calls=%async_computation.3 | async-start | bytes 2097152 | tf_op jit(solution)/shard_map/all_to_all | solution.py:157
Sparse Core Ops, SparseCore 0:
  22.7 127.6 reduce-scatter.1
  153.1 49.3 all-gather.1
  205.4 21.2 all-reduce.2
  275.1 20.4 all-reduce.4
where the time goes:
time: 343 us; the launch traced here: 340 us
  waiting for transfers between devices  232 us (68%)
  blocking collectives  30.4 us (9%)
  matrix products  20.2 us (6%)
  local copies, waits for them, and re-layouts  15.4 us (4%)
  other arithmetic  14.3 us (4%)
  between operations  14 us (4%)
  starting transfers between devices  13 us (4%)
    reduce_scatter x1, waiting for transfers between devices, body(): lax.psum_scatter(jnp.dot(spread, joined, preferred_element_type=jnp.float...  127 us
    all_gather x1, waiting for transfers between devices, body(): lax.all_gather(w_out, 'ep', axis=1, tiled=True)  38.4 us
    all_to_all x1, blocking collectives, body(): lax.all_to_all(outgoing, 'ep', split_axis=0, concat_axis=0, tiled=True)  30.4 us
    all_to_all x1, waiting for transfers between devices, body(): lax.all_to_all(finished, 'ep', split_axis=0, concat_axis=0, tiled=True)  23.3 us
    psum x1, waiting for transfers between devices, body(): lax.psum(partial_out.astype(jnp.bfloat16), 'tp').astype(jnp.float32)  21.4 us
    psum x1, waiting for transfers between devices, body(): expert_sum = lax.psum(partial_down.astype(jnp.bfloat16), 'tp')  20.7 us
  transfers between devices with their start and end apart: 6, of which 6 were waited for; matrix products, arithmetic and copies ran while one was open for 5% of the time, Pallas kernels for 0%

commit v1 on v0

--- a/solution.py
+++ b/solution.py
@@ -1,7 +1,475 @@
+import functools
+
 import jax
 import jax.numpy as jnp
 from jax import lax
+from jax.experimental import pallas as pl
+from jax.experimental.pallas import tpu as pltpu
 from jax.sharding import PartitionSpec as P
+
+MESH = pl.DeviceIdType.MESH
+PLANE = 4
+LANES = 128
+SLOT_TILE = 16
+VMEM_BYTES = 60 * 1024 * 1024
+
+
+def remote(src, dst, send_sem, recv_sem, target):
+    return pltpu.make_async_remote_copy(
+        src_ref=src,
+        dst_ref=dst,
+        send_sem=send_sem,
+        recv_sem=recv_sem,
+        device_id=target,
+        device_id_type=MESH,
+    )
+
+
+def dot_t(left, right):
+    return lax.dot_general(
+        left, right, (((1,), (1,)), ((), ())), preferred_element_type=jnp.float32
+    )
+
+
+def mixer_kernel(
+    lines,
+    tokens_ref,
+    gain_ref,
+    wq_ref,
+    wk_ref,
+    wv_ref,
+    wo_gate_ref,
+    gates_ref,
+    w_out_ref,
+    proj_ref,
+    w_all_ref,
+    normed,
+    spread,
+    weights,
+    partial,
+    outgoing,
+    arrived,
+    local_sem,
+    w_send,
+    w_recv,
+    x_send,
+    x_recv,
+    p_send,
+    p_recv,
+    z_send,
+    z_recv,
+    o_send,
+    o_recv,
+):
+    ep, tp = lax.axis_index("ep"), lax.axis_index("tp")
+    line, spot = ep // PLANE, ep % PLANE
+    rows, width = tokens_ref.shape
+    depth = wq_ref.shape[0]
+    block = depth * PLANE
+
+    def line_peer(step):
+        other = lax.rem(line + step, lines)
+        return other, (other * PLANE + spot, tp)
+
+    def plane_peer(step):
+        return (line * PLANE + lax.rem(spot + step, PLANE), tp)
+
+    own_rows = pl.ds(pl.multiple_of(spot * depth, depth), depth)
+    copies = []
+    start = 0
+    for index, ref in enumerate((wq_ref, wk_ref, wv_ref, wo_gate_ref, gates_ref)):
+        columns = ref.shape[1]
+        copy = pltpu.make_async_copy(
+            ref, weights.at[own_rows, start : start + columns], local_sem.at[index]
+        )
+        copy.start()
+        copies.append(copy)
+        start += columns
+    keep_out = pltpu.make_async_copy(w_out_ref, w_all_ref.at[spot, line], local_sem.at[5])
+    keep_out.start()
+    barrier = pltpu.get_barrier_semaphore()
+    for step in range(1, lines):
+        pl.semaphore_signal(barrier, inc=1, device_id=line_peer(step)[1], device_id_type=MESH)
+    for step in range(1, PLANE):
+        pl.semaphore_signal(barrier, inc=1, device_id=plane_peer(step), device_id_type=MESH)
+    widened = tokens_ref[...].astype(jnp.float32)
+    scale = lax.rsqrt(jnp.mean(widened * widened, axis=-1, keepdims=True) + 1e-06)
+    normed[...] = (widened * scale * gain_ref[...]).astype(jnp.bfloat16)
+    pl.semaphore_wait(barrier, lines - 1 + PLANE - 1)
+    for copy in copies:
+        copy.wait()
+    w_copies, x_copies, z_copies, p_copies, o_copies = [], [], [], [], []
+    for step in range(1, PLANE):
+        copy = remote(
+            weights.at[own_rows],
+            weights.at[own_rows],
+            w_send.at[step],
+            w_recv.at[step],
+            plane_peer(step),
+        )
+        copy.start()
+        w_copies.append(copy)
+    for step in range(1, lines):
+        other, target = line_peer(step)
+        copy = remote(
+            normed.at[:, pl.ds(pl.multiple_of(other * block, block), block)],
+            spread.at[line],
+            x_send.at[step],
+            x_recv.at[step],
+            target,
+        )
+        copy.start()
+        x_copies.append(copy)
+    for step in range(1, lines):
+        copy = remote(
+            w_out_ref,
+            w_all_ref.at[spot, line],
+            z_send.at[step],
+            z_recv.at[step],
+            line_peer(step)[1],
+        )
+        copy.start()
+        z_copies.append(copy)
+    spread[line] = normed[:, pl.ds(pl.multiple_of(line * block, block), block)]
+    keep_out.wait()
+    for copy in x_copies:
+        copy.wait()
+    for copy in z_copies:
+        copy.wait()
+    for step in range(1, PLANE):
+        copy = remote(
+            w_all_ref.at[spot],
+            w_all_ref.at[spot],
+            o_send.at[step],
+            o_recv.at[step],
+            plane_peer(step),
+        )
+        copy.start()
+        o_copies.append(copy)
+    for copy in w_copies:
+        copy.wait()
+    main = weights.shape[1] - LANES
+    product = jnp.dot(
+        spread[...].reshape(lines * rows, block),
+        weights[...],
+        preferred_element_type=jnp.float32,
+    )
+    outgoing[:, :, :main] = product[:, :main].astype(jnp.bfloat16).reshape(lines, rows, main)
+    gates = product[:, main:]
+    coarse = gates.astype(jnp.bfloat16)
+    fine = (gates - coarse.astype(jnp.float32)).astype(jnp.bfloat16)
+    first = lax.broadcasted_iota(jnp.int32, gates.shape, 1) < LANES // 2
+    picked = jnp.where(first, coarse.astype(jnp.float32), fine.astype(jnp.float32))
+    outgoing[:, :, main:] = picked.astype(jnp.bfloat16).reshape(lines, rows, LANES)
+    partial[:, :, :main] = product[:, :main].reshape(lines, rows, main)
+    partial[:, :, main:] = jnp.where(first, gates, 0.0).reshape(lines, rows, LANES)
+    for step in range(1, lines):
+        other, target = line_peer(step)
+        copy = remote(
+            outgoing.at[other], arrived.at[step], p_send.at[step], p_recv.at[step], target
+        )
+        copy.start()
+        p_copies.append(copy)
+    total = partial[line]
+    for step in range(1, lines):
+        p_copies[step - 1].wait()
+        total = total + arrived[step].astype(jnp.float32)
+    proj_ref[...] = total
+    for copy in o_copies:
+        copy.wait()
+
+
+def expert_kernel(
+    count,
+    cell_ref,
+    w_all_ref,
+    tokens_ref,
+    gain_ref,
+    target_rows_ref,
+    target_cols_ref,
+    route_weights_ref,
+    w_gate_hbm,
+    w_up_hbm,
+    w_down_hbm,
+    mixed_ref,
+    w_gate,
+    w_up,
+    w_down,
+    mine,
+    theirs,
+    resid,
+    outgoing,
+    near,
+    far,
+    down_send,
+    down_recv,
+    finished,
+    returned,
+    last_send,
+    last_recv,
+    local_sem,
+    t_send,
+    t_recv,
+    d_send,
+    d_recv,
+    f_send,
+    f_recv,
+    r_send,
+    r_recv,
+):
+    ep, tp = lax.axis_index("ep"), lax.axis_index("tp")
+    partner = (ep, 1 - tp)
+    rows, width = tokens_ref.shape
+    half = width // 2
+    slots = count * SLOT_TILE
+    top = route_weights_ref.shape[1]
+    loads = []
+    for index, (source, kept) in enumerate(
+        ((w_gate_hbm, w_gate), (w_up_hbm, w_up), (w_down_hbm, w_down))
+    ):
+        copy = pltpu.make_async_copy(source, kept, local_sem.at[index])
+        copy.start()
+        loads.append(copy)
+    barrier = pltpu.get_barrier_semaphore()
+    for step in range(1, count):
+        pl.semaphore_signal(
+            barrier, inc=1, device_id=(lax.rem(ep + step, count), tp), device_id_type=MESH
+        )
+    pl.semaphore_signal(barrier, inc=1, device_id=partner, device_id_type=MESH)
+    cell = cell_ref[...]
+    columns = w_all_ref.shape[3]
+    lines = w_all_ref.shape[1]
+    for line in range(lines):
+        for spot in range(PLANE):
+            start = (line * PLANE + spot) * columns
+            mine[:, start : start + columns] = jnp.dot(
+                cell, w_all_ref[spot, line], preferred_element_type=jnp.float32
+            ).astype(jnp.bfloat16)
+    pl.semaphore_wait(barrier, count)
+    swap = remote(mine, theirs, t_send.at[0], t_recv.at[0], partner)
+    swap.start()
+    slot_row = lax.broadcasted_iota(jnp.int32, (slots, rows), 0)
+    dispatch = jnp.zeros((slots, rows), jnp.float32)
+    for k in range(top):
+        dispatch += jnp.where(slot_row == target_rows_ref[k : k + 1, :], 1.0, 0.0)
+    dispatch = dispatch.astype(jnp.bfloat16)
+    swap.wait()
+    summed = mine[...].astype(jnp.float32) + theirs[...].astype(jnp.float32)
+    resid[...] = (tokens_ref[...].astype(jnp.float32) + summed).astype(jnp.bfloat16)
+    widened = resid[...].astype(jnp.float32)
+    scale = lax.rsqrt(jnp.mean(widened * widened, axis=-1, keepdims=True) + 1e-06)
+    my_half = pl.ds(pl.multiple_of(tp * half, half), half)
+    other_half = pl.ds(pl.multiple_of((1 - tp) * half, half), half)
+    normed = (resid[:, my_half].astype(jnp.float32) * scale * gain_ref[:, my_half]).astype(
+        jnp.bfloat16
+    )
+    outgoing[...] = (
+        jnp.dot(dispatch, normed, preferred_element_type=jnp.float32)
+        .astype(jnp.bfloat16)
+        .reshape(count, SLOT_TILE, half)
+    )
+    sends = []
+    for step in range(1, count):
+        other = lax.rem(ep + step, count)
+        copy = remote(
+            outgoing.at[other], near.at[ep], d_send.at[step], d_recv.at[step], (other, tp)
+        )
+        copy.start()
+        sends.append(copy)
+    near[ep] = outgoing[ep]
+    forwards = []
+    for step in range(count):
+        source = lax.rem(ep + count - step, count)
+        if step > 0:
+            sends[step - 1].wait()
+        copy = remote(
+            near.at[source] if step > 0 else outgoing.at[ep],
+            far.at[source],
+            f_send.at[step],
+            f_recv.at[step],
+            partner,
+        )
+        copy.start()
+        forwards.append(copy)
+    for copy in loads:
+        copy.wait()
+    near_rows = near[...].reshape(slots, half)
+    gate_pre = dot_t(near_rows, w_gate[:, my_half])
+    up_pre = dot_t(near_rows, w_up[:, my_half])
+    for copy in forwards:
+        copy.wait()
+    far_rows = far[...].reshape(slots, half)
+    gate_pre += dot_t(far_rows, w_gate[:, other_half])
+    up_pre += dot_t(far_rows, w_up[:, other_half])
+    hidden = (gate_pre * jax.nn.sigmoid(gate_pre) * up_pre).astype(jnp.bfloat16)
+    down_send[...] = jnp.dot(
+        hidden, w_down[:, other_half], preferred_element_type=jnp.float32
+    ).astype(jnp.bfloat16)
+    swap = remote(down_send, down_recv, t_send.at[1], t_recv.at[1], partner)
+    swap.start()
+    kept = jnp.dot(hidden, w_down[:, my_half], preferred_element_type=jnp.float32).astype(
+        jnp.bfloat16
+    )
+    swap.wait()
+    finished[...] = (
+        (kept.astype(jnp.float32) + down_recv[...].astype(jnp.float32))
+        .astype(jnp.bfloat16)
+        .reshape(count, SLOT_TILE, half)
+    )
+    sends = []
+    for step in range(1, count):
+        other = lax.rem(ep + step, count)
+        copy = remote(
+            finished.at[other], returned.at[ep], r_send.at[step], r_recv.at[step], (other, tp)
+        )
+        copy.start()
+        sends.append(copy)
+    returned[ep] = finished[ep]
+    slot_col = lax.broadcasted_iota(jnp.int32, (rows, slots), 1)
+    combine = jnp.zeros((rows, slots), jnp.float32)
+    for k in range(top):
+        combine += jnp.where(
+            slot_col == target_cols_ref[:, k : k + 1], route_weights_ref[:, k : k + 1], 0.0
+        )
+    coarse = combine.astype(jnp.bfloat16)
+    fine = (combine - coarse.astype(jnp.float32)).astype(jnp.bfloat16)
+    for copy in sends:
+        copy.wait()
+    back = returned[...].reshape(slots, half)
+    weighted = jnp.dot(coarse, back, preferred_element_type=jnp.float32) + jnp.dot(
+        fine, back, preferred_element_type=jnp.float32
+    )
+    last_send[...] = (resid[:, my_half].astype(jnp.float32) + weighted).astype(jnp.bfloat16)
+    swap = remote(last_send, last_recv, t_send.at[2], t_recv.at[2], partner)
+    swap.start()
+    mixed_ref[:, my_half] = last_send[...]
+    swap.wait()
+    mixed_ref[:, other_half] = last_recv[...]
+
+
+def mixer_call(tokens, mix_gain, weight_list, w_out):
+    rows, width = tokens.shape
+    w_query, w_key, w_value, w_outgate, w_igate, w_fgate = weight_list
+    depth, columns = w_query.shape
+    lines = lax.axis_size("ep") // PLANE
+    heads = w_igate.shape[1]
+    pair = jnp.concatenate((w_igate, w_fgate), axis=1)
+    pad = jnp.zeros((depth, LANES // 2 - 2 * heads), pair.dtype)
+    gates = jnp.concatenate((pair, pad, pair, pad), axis=1)
+    total = 4 * columns + LANES
+    vmem = pl.BlockSpec(memory_space=pltpu.VMEM)
+    anywhere = pl.BlockSpec(memory_space=pl.ANY)
+    dma = pltpu.SemaphoreType.DMA
+    proj, w_all = pl.pallas_call(
+        functools.partial(mixer_kernel, lines),
+        out_shape=(
+            jax.ShapeDtypeStruct((rows, total), jnp.float32),
+            jax.ShapeDtypeStruct((PLANE, lines) + w_out.shape, jnp.bfloat16),
+        ),
+        in_specs=[vmem, vmem] + [anywhere] * 5 + [vmem],
+        out_specs=(vmem, anywhere),
+        scratch_shapes=[
+            pltpu.VMEM((rows, width), jnp.bfloat16),
+            pltpu.VMEM((lines, rows, depth * PLANE), jnp.bfloat16),
+            pltpu.VMEM((depth * PLANE, total), jnp.bfloat16),
+            pltpu.VMEM((lines, rows, total), jnp.float32),
+            pltpu.VMEM((lines, rows, total), jnp.bfloat16),
+            pltpu.VMEM((lines, rows, total), jnp.bfloat16),
+            dma((6,)),
+            dma((PLANE,)),
+            dma((PLANE,)),
+            dma((lines,)),
+            dma((lines,)),
+            dma((lines,)),
+            dma((lines,)),
+            dma((lines,)),
+            dma((lines,)),
+            dma((PLANE,)),
+            dma((PLANE,)),
+        ],
+        compiler_params=pltpu.CompilerParams(
+            collective_id=0, has_side_effects=True, vmem_limit_bytes=16 * 1024 * 1024
+        ),
+    )(tokens, mix_gain[None, :], w_query, w_key, w_value, w_outgate, gates, w_out)
+    main = 4 * columns
+    gate_sums = proj[:, main : main + LANES // 2] + proj[:, main + LANES // 2 :]
+    return (
+        proj[:, :columns],
+        proj[:, columns : 2 * columns],
+        proj[:, 2 * columns : 3 * columns],
+        proj[:, 3 * columns : main],
+        gate_sums[:, :heads],
+        gate_sums[:, heads : 2 * heads],
+    ), w_all
+
+
+def expert_call(
+    cell_out, w_all, tokens, ffn_gain, routes, route_weights, w_gate, w_up, w_down
+):
+    rows, width = tokens.shape
+    count = lax.axis_size("ep")
+    flat = routes.reshape(-1)
+    same = (flat[:, None] == flat[None, :]).astype(jnp.int32)
+    order = jnp.arange(flat.shape[0], dtype=jnp.int32)
+    earlier = (order[None, :] < order[:, None]).astype(jnp.int32)
+    slots = jnp.sum(same * earlier, axis=1, dtype=jnp.int32)
+    targets = (flat * SLOT_TILE + slots).reshape(routes.shape)
+    gate_t = jnp.swapaxes(w_gate[0], 0, 1)
+    up_t = jnp.swapaxes(w_up[0], 0, 1)
+    down = w_down[0]
+    half = width // 2
+    area = count * SLOT_TILE
+    vmem = pl.BlockSpec(memory_space=pltpu.VMEM)
+    anywhere = pl.BlockSpec(memory_space=pl.ANY)
+    dma = pltpu.SemaphoreType.DMA
+    bf = jnp.bfloat16
+    tile = (count, SLOT_TILE, half)
+    return pl.pallas_call(
+        functools.partial(expert_kernel, count),
+        out_shape=jax.ShapeDtypeStruct((rows, width), bf),
+        in_specs=[vmem] * 7 + [anywhere] * 3,
+        out_specs=vmem,
+        scratch_shapes=[
+            pltpu.VMEM(gate_t.shape, bf),
+            pltpu.VMEM(up_t.shape, bf),
+            pltpu.VMEM(down.shape, bf),
+            pltpu.VMEM((rows, width), bf),
+            pltpu.VMEM((rows, width), bf),
+            pltpu.VMEM((rows, width), bf),
+            pltpu.VMEM(tile, bf),
+            pltpu.VMEM(tile, bf),
+            pltpu.VMEM(tile, bf),
+            pltpu.VMEM((area, half), bf),
+            pltpu.VMEM((area, half), bf),
+            pltpu.VMEM(tile, bf),
+            pltpu.VMEM(tile, bf),
+            pltpu.VMEM((rows, half), bf),
+            pltpu.VMEM((rows, half), bf),
+            dma((3,)),
+            dma((3,)),
+            dma((3,)),
+            dma((count,)),
+            dma((count,)),
+            dma((count,)),
+            dma((count,)),
+            dma((count,)),
+            dma((count,)),
+        ],
+        compiler_params=pltpu.CompilerParams(
+            collective_id=1, has_side_effects=True, vmem_limit_bytes=40 * 1024 * 1024
+        ),
+    )(
+        cell_out,
+        w_all,
+        tokens,
+        ffn_gain[None, :],
+        jnp.swapaxes(targets, 0, 1),
+        targets,
+        route_weights,
+        gate_t,
+        up_t,
+        down,
+    )
 
 
 def rms_scale(values_in, gain_vec):
@@ -53,6 +521,24 @@
     return (cell_out, new_matrix, new_norm, new_max)
 
 
+def kernels_fit(tokens, w_query, w_igate, w_out, w_expert_gate, routes):
+    ep_count = lax.axis_size("ep")
+    rows, width = tokens.shape
+    capacity = max(2, 2 * rows * routes.shape[1] // (w_expert_gate.shape[0] * ep_count))
+    return (
+        lax.axis_size("tp") == 2
+        and ep_count % PLANE == 0
+        and w_query.shape[0] % LANES == 0
+        and w_query.shape[1] % LANES == 0
+        and w_out.shape[1] % LANES == 0
+        and width % (2 * LANES) == 0
+        and rows % SLOT_TILE == 0
+        and w_igate.shape[1] * 4 <= LANES
+        and w_expert_gate.shape[0] == 1
+        and capacity <= SLOT_TILE
+    )
+
+
 def body(
     tokens,
     mix_gain,
@@ -77,8 +563,34 @@
     route_weights,
 ):
     seq_rows, width = tokens.shape
+    weight_list = (w_query, w_key, w_value, w_outgate, w_igate, w_fgate)
+    if kernels_fit(tokens, w_query, w_igate, w_out, w_expert_gate, routes):
+        projected, w_all = mixer_call(tokens, mix_gain, weight_list, w_out)
+        cell_out, new_matrix, new_norm, new_max = memory_cell(
+            projected[0].astype(jnp.bfloat16),
+            projected[1].astype(jnp.bfloat16),
+            projected[2].astype(jnp.bfloat16),
+            projected[3].astype(jnp.bfloat16),
+            projected[4] + igate_bias,
+            projected[5] + fgate_bias,
+            head_gain,
+            state_matrix,
+            state_norm,
+            state_max,
+        )
+        mixed = expert_call(
+            cell_out,
+            w_all,
+            tokens,
+            ffn_gain,
+            routes,
+            route_weights,
+            w_expert_gate,
+            w_expert_up,
+            w_expert_down,
+        )
+        return (mixed, new_matrix, new_norm, new_max)
     normed = rms_scale(tokens, mix_gain).astype(jnp.bfloat16)
-    weight_list = (w_query, w_key, w_value, w_outgate, w_igate, w_fgate)
     spread = lax.all_to_all(normed, "ep", split_axis=1, concat_axis=0, tiled=True)
     joined = jnp.concatenate(weight_list, axis=1)
     summed = lax.psum_scatter(

time: 343 us -> 102 us (0.30)
  waiting for transfers between devices: 232 us -> 0 us
  Pallas kernels: 0 us -> 68.7 us
  blocking collectives: 30.4 us -> 0 us
  matrix products: 20.2 us -> 5.7 us
  between operations: 14 us -> 0.85 us
  starting transfers between devices: 13 us -> 0 us
  other arithmetic: 14.3 us -> 9.86 us
    reduce_scatter x1 -> x0, waiting for transfers between devices: 127 us -> none  [body(): lax.psum_scatter(jnp.dot(spread, joined, preferred_element_type=jnp.float...]
    pallas_call x0 -> x2, Pallas kernels: none -> 68.7 us  [the longest x1 40.7 us: expert_call(): pl.pallas_call(functools.partial(expert_kernel, count), out_shape=jax.Sha...]
    psum x2 -> x0, waiting for transfers between devices: 42.1 us -> none  [the longest x1 21.4 us: body(): lax.psum(partial_out.astype(jnp.bfloat16), 'tp').astype(jnp.float32)]
    all_gather x1 -> x0, waiting for transfers between devices: 38.4 us -> none  [body(): lax.all_gather(w_out, 'ep', axis=1, tiled=True)]
    all_to_all x1 -> x0, blocking collectives: 30.4 us -> none  [body(): lax.all_to_all(outgoing, 'ep', split_axis=0, concat_axis=0, tiled=True)]
    all_to_all x2 -> x0, waiting for transfers between devices: 24.4 us -> none  [the longest x1 23.3 us: body(): lax.all_to_all(finished, 'ep', split_axis=0, concat_axis=0, tiled=True)]
    dot_general x6 -> x0, matrix products: 16.9 us -> none  [the longest x1 5.2 us: body(): jnp.einsum('nxcf,xfd->nxcd', hidden, w_expert_down, preferred_element_typ...]
    all_to_all x2 -> x0, starting transfers between devices: 12.9 us -> none  [the longest x1 6.49 us: body(): lax.all_to_all(finished, 'ep', split_axis=0, concat_axis=0, tiled=True)]
  transfers between devices with their start and end apart: 6 -> 0, of which waited for: 6 -> 0; matrix products, arithmetic and copies ran while one was open for 5% -> 0% of each run, Pallas kernels for 0% -> 0%
where the time goes in v1:
time: 102 us
  Pallas kernels  68.7 us (67%)
  local copies, waits for them, and re-layouts  16.5 us (16%)
  other arithmetic  9.86 us (10%)
  matrix products  5.7 us (6%)
    pallas_call x1, Pallas kernels, expert_call(): pl.pallas_call(functools.partial(expert_kernel, count), out_shape=jax.Sha...  40.7 us
    pallas_call x1, Pallas kernels, mixer_call(): pl.pallas_call(functools.partial(mixer_kernel, lines), out_shape=(jax.Sha...  28 us
    unnamed x41, local copies, waits for them, and re-layouts  15.5 us
    add x1, other arithmetic, memory_cell(): keep_old[:, :, None, None] * state_matrix  5.88 us
    dot_general x1, matrix products, memory_cell(): jnp.einsum('bhvd,bhd->bhv', new_matrix, query_heads, precision=lax.Precis...  5.7 us

profile of v1, /device:TPU:29, one launch (start us, length us, event | category | flops | bytes accessed | tf_op | source)
XLA Modules:
  0.0 101.6 jit_solution(457820473938768722)
XLA Ops:
  0.6 0.8 copy.58
  1.4 0.8 copy.59
  2.4 0.9 copy-done.5
  3.3 0.8 copy-done.7
  4.1 0.8 copy-done.8
  5.0 0.8 copy-done.9
  5.8 0.8 copy-done.10
  6.7 0.8 copy-done.11
  7.5 0.7 copy-done.12
  8.2 28.0 %shard_map.228 = (f32[32,1152]{1,0:T(8,128)S(1)}, bf16[4,4,256,128]{3,2,1,0:T(8,128)(2,1)S(1)}) custom-call(bf16[32,2048]{1,0:T(8,128)(2,1)S(1)} %copy-done.5, f32[1,2048]{1,0:T(1,128)S(1)} %bitcast.18, bf16[128,256]{1,0:T(8,128)(2,1)S(1)} %copy-done.7, bf16[128,256]{1,0:T(8,128)(2,1)S(1)} %copy-done.8, bf16[128,256]{1,0:T(8,128)(2,1)S(1)} %copy-done.9, ...), custom_call_target="tpu_custom_call" | custom-call | tf_op jit(solution)/shard_map/pallas_call | solution.py:363
  36.2 1.0 copy-done.3
  37.2 0.8 copy.62
  38.0 0.8 broadcast_multiply_fusion.3
  38.8 0.8 subtract_exponential_fusion.1
  39.8 1.6 %multiply_reduce_fusion.1 = (f32[32,4]{1,0:T(8,128)S(1)}, f32[32,4,64]{2,1,0:T(4,128)}, f32[32,4,64]{2,1,0:T(4,128)S(1)}, f32[32,4,64]{2,1,0:T(4,128)S(1)}) fusion(bf16[32,4,64]{2,1,0:T(4,128)(2,1)S(1)} %reshape.65, f32[32,4,64]{2,1,0:T(4,128)S(1)} %reshape.70, f32[32,4]{1,0:T(8,128)S(1)} %get-tuple-element.28, f32[32,4,64]{2,1,0:T(4,128)} %param.34, ...), kind=kLoop, calls=%fused_computation.2 | loop fusion | flops 65408 | bytes 215040 | tf_op jit(solution)/shard_map/reduce_sum | solution.py:513
  41.5 5.9 %multiply_add_fusion = f32[32,4,64,64]{3,2,1,0:T(8,128)} fusion(f32[32,4,64,64]{3,2,1,0:T(8,128)} %param.33, f32[32,4,64]{2,1,0:T(4,128)S(1)} %get-tuple-element.34, f32[32,4,64]{2,1,0:T(4,128)S(1)} %get-tuple-element.35, f32[32,4]{1,0:T(8,128)S(1)} %subtract_exponential_fusion.1), kind=kLoop, calls=%fused_computation | loop fusion | flops 1572864 | bytes 4260352 | tf_op jit(solution)/shard_map/add | solution.py:506
  47.5 5.7 %fusion.7 = f32[32,4,1,64]{3,2,1,0:T(1,128)S(1)} fusion(f32[32,4,64,64]{3,2,1,0:T(8,128)} %multiply_add_fusion, bf16[32,4,64,1]{2,3,1,0:T(2,128)(2,1)S(1)} %reshape.74), kind=kOutput, calls=%fused_computation.30 | convolution fusion | flops 6291456 | bytes 2146304 | tf_op jit(solution)/shard_map/bhvd,bhd->bhv/dot_general | solution.py:510
  53.2 0.2 fusion.4
  54.7 1.8 %copy-done.1 = bf16[1,2048,704]{1,2,0:T(8,128)(2,1)S(1)} copy-done((bf16[1,2048,704]{1,2,0:T(8,128)(2,1)S(1)}, bf16[1,2048,704]{1,2,0:T(8,128)(2,1)}, u32[]{:S(2)}) %copy-start.1) | copy-done | bytes 2883608
  56.5 1.8 %copy-done.2 = bf16[1,704,2048]{2,1,0:T(8,128)(2,1)S(1)} copy-done((bf16[1,704,2048]{2,1,0:T(8,128)(2,1)S(1)}, bf16[1,704,2048]{2,1,0:T(8,128)(2,1)}, u32[]{:S(2)}) %copy-start.2) | copy-done | bytes 2883608
  58.3 1.2 %copy-done.4 = bf16[4,4,256,128]{3,2,1,0:T(8,128)(2,1)S(1)} copy-done((bf16[4,4,256,128]{3,2,1,0:T(8,128)(2,1)S(1)}, bf16[4,4,256,128]{3,2,1,0:T(8,128)(2,1)}, u32[]{:S(2)}) %copy-start.4) | copy-done | bytes 1048600
  59.5 40.7 %shard_map.229 = bf16[32,2048]{1,0:T(8,128)(2,1)S(1)} custom-call(bf16[32,256]{1,0:T(8,128)(2,1)S(1)} %multiply_convert_fusion.cell_ref, bf16[4,4,256,128]{3,2,1,0:T(8,128)(2,1)S(1)} %copy-done.4, bf16[32,2048]{1,0:T(8,128)(2,1)S(1)} %copy-done.6, f32[1,2048]{1,0:T(1,128)S(1)} %bitcast.19, s32[3,32]{1,0:T(4,128)S(1)} %copy.65.target_rows_ref, ...), custom_call_target="tpu_custom_call" | custom-call | tf_op jit(solution)/shard_map/pallas_call | solution.py:427
  100.3 0.7 copy.67
  100.9 0.7 copy.71
  (48 shorter events, 1.9 us)
Async XLA Ops:
  2.4 0.9 copy-start.5
  3.3 0.8 copy-start.7
  4.1 0.8 copy-start.8
  5.0 0.8 copy-start.9
  5.8 0.8 copy-start.10
  6.7 0.8 copy-start.11
  7.5 0.7 copy-start.12
  36.2 1.0 copy-start.3
  47.4 6.5 %copy-start.16 = (f32[256]{0:T(256)S(1)}, f32[256]{0:T(256)}, u32[]{:S(2)}) copy-start(f32[256]{0:T(256)} %param.31) | copy-start | bytes 3076
  47.4 6.5 %copy-start.14 = (s32[32,3]{0,1:T(4,128)S(1)}, s32[32,3]{0,1:T(4,128)}, u32[]{:S(2)}) copy-start(s32[32,3]{0,1:T(4,128)} %param.40) | copy-start | bytes 1156
  47.4 7.2 %copy-start.15 = (f32[32,3]{0,1:T(4,128)S(1)}, f32[32,3]{0,1:T(4,128)}, u32[]{:S(2)}) copy-start(f32[32,3]{0,1:T(4,128)} %param.41) | copy-start | bytes 1156
  47.4 7.3 %copy-start = (bf16[1,2048,704]{1,2,0:T(8,128)(2,1)S(1)}, bf16[1,2048,704]{1,2,0:T(8,128)(2,1)}, u32[]{:S(2)}) copy-start(bf16[1,2048,704]{1,2,0:T(8,128)(2,1)} %param.37) | copy-start | bytes 8650756
  47.4 7.3 %copy-start.6 = (bf16[32,2048]{1,0:T(8,128)(2,1)S(1)}, bf16[32,2048]{1,0:T(8,128)(2,1)}, u32[]{:S(2)}) copy-start(bf16[32,2048]{1,0:T(8,128)(2,1)} %tokens_ref.3) | copy-start | bytes 393220
  47.4 7.3 %copy-start.13 = (f32[2048]{0:T(1024)S(1)}, f32[2048]{0:T(1024)}, u32[]{:S(2)}) copy-start(f32[2048]{0:T(1024)} %param.36) | copy-start | bytes 24580
  54.7 1.8 %copy-start.1 = (bf16[1,2048,704]{1,2,0:T(8,128)(2,1)S(1)}, bf16[1,2048,704]{1,2,0:T(8,128)(2,1)}, u32[]{:S(2)}) copy-start(bf16[1,2048,704]{1,2,0:T(8,128)(2,1)} %param.38) | copy-start | bytes 8650756
  56.5 1.8 %copy-start.2 = (bf16[1,704,2048]{2,1,0:T(8,128)(2,1)S(1)}, bf16[1,704,2048]{2,1,0:T(8,128)(2,1)}, u32[]{:S(2)}) copy-start(bf16[1,704,2048]{2,1,0:T(8,128)(2,1)} %param.39) | copy-start | bytes 8650756
  58.3 1.2 %copy-start.4 = (bf16[4,4,256,128]{3,2,1,0:T(8,128)(2,1)S(1)}, bf16[4,4,256,128]{3,2,1,0:T(8,128)(2,1)}, u32[]{:S(2)}) copy-start(bf16[4,4,256,128]{3,2,1,0:T(8,128)(2,1)} %copy-done.3) | copy-start | bytes 3145732

commit v2 on v1

--- a/solution.py
+++ b/solution.py
@@ -31,18 +31,34 @@
     )
 
 
+def fetch_all(pairs, sems):
+    copies = []
+    for index, (source, kept) in enumerate(pairs):
+        copy = pltpu.make_async_copy(source, kept, sems.at[index])
+        copy.start()
+        copies.append(copy)
+    return copies
+
+
 def mixer_kernel(
     lines,
-    tokens_ref,
-    gain_ref,
+    tokens_hbm,
+    gain_hbm,
     wq_ref,
     wk_ref,
     wv_ref,
     wo_gate_ref,
-    gates_ref,
-    w_out_ref,
+    igate_hbm,
+    fgate_hbm,
+    w_out_hbm,
     proj_ref,
     w_all_ref,
+    tokens_ref,
+    gain_ref,
+    igate_ref,
+    fgate_ref,
+    turned,
+    w_planes,
     normed,
     spread,
     weights,
@@ -66,49 +82,91 @@
     rows, width = tokens_ref.shape
     depth = wq_ref.shape[0]
     block = depth * PLANE
+    heads = igate_ref.shape[0]
+    beside = spot + 1 - 2 * (spot % 2)
+    across = lax.rem(spot + 2, PLANE)
+    beside_peer = (line * PLANE + beside, tp)
+    across_peer = (line * PLANE + across, tp)
 
     def line_peer(step):
         other = lax.rem(line + step, lines)
         return other, (other * PLANE + spot, tp)
 
-    def plane_peer(step):
-        return (line * PLANE + lax.rem(spot + step, PLANE), tp)
-
     own_rows = pl.ds(pl.multiple_of(spot * depth, depth), depth)
-    copies = []
+    pairs = [
+        (tokens_hbm, tokens_ref),
+        (gain_hbm, gain_ref),
+        (igate_hbm, igate_ref),
+        (fgate_hbm, fgate_ref),
+        (w_out_hbm, w_planes.at[spot, line]),
+    ]
     start = 0
-    for index, ref in enumerate((wq_ref, wk_ref, wv_ref, wo_gate_ref, gates_ref)):
+    for ref in (wq_ref, wk_ref, wv_ref, wo_gate_ref):
         columns = ref.shape[1]
-        copy = pltpu.make_async_copy(
-            ref, weights.at[own_rows, start : start + columns], local_sem.at[index]
-        )
-        copy.start()
-        copies.append(copy)
+        pairs.append((ref, weights.at[own_rows, start : start + columns]))
         start += columns
-    keep_out = pltpu.make_async_copy(w_out_ref, w_all_ref.at[spot, line], local_sem.at[5])
-    keep_out.start()
+    main = start
+    copies = fetch_all(pairs, local_sem)
     barrier = pltpu.get_barrier_semaphore()
     for step in range(1, lines):
         pl.semaphore_signal(barrier, inc=1, device_id=line_peer(step)[1], device_id_type=MESH)
-    for step in range(1, PLANE):
-        pl.semaphore_signal(barrier, inc=1, device_id=plane_peer(step), device_id_type=MESH)
+    pl.semaphore_signal(barrier, inc=1, device_id=beside_peer, device_id_type=MESH)
+    pl.semaphore_signal(barrier, inc=1, device_id=across_peer, device_id_type=MESH)
+    turned[...] = jnp.zeros_like(turned)
+    for copy in copies:
+        copy.wait()
+    for place in (0, LANES // 2):
+        turned[place : place + heads, :] = igate_ref[...].astype(jnp.float32)
+        turned[place + heads : place + 2 * heads, :] = fgate_ref[...].astype(jnp.float32)
+    weights[own_rows, main:] = turned[...].T.astype(jnp.bfloat16)
     widened = tokens_ref[...].astype(jnp.float32)
     scale = lax.rsqrt(jnp.mean(widened * widened, axis=-1, keepdims=True) + 1e-06)
     normed[...] = (widened * scale * gain_ref[...]).astype(jnp.bfloat16)
-    pl.semaphore_wait(barrier, lines - 1 + PLANE - 1)
-    for copy in copies:
-        copy.wait()
-    w_copies, x_copies, z_copies, p_copies, o_copies = [], [], [], [], []
-    for step in range(1, PLANE):
-        copy = remote(
-            weights.at[own_rows],
-            weights.at[own_rows],
-            w_send.at[step],
-            w_recv.at[step],
-            plane_peer(step),
-        )
-        copy.start()
-        w_copies.append(copy)
+    pl.semaphore_wait(barrier, lines - 1 + 2)
+
+    def row_part(owner, part):
+        size = depth // 2
+        return pl.ds(pl.multiple_of(owner * depth + part * size, size), size)
+
+    def w_copy(owner, part, slot, target):
+        view = weights.at[row_part(owner, part)]
+        return remote(view, view, w_send.at[slot], w_recv.at[slot], target)
+
+    def o_copy(owner, part, slot, target):
+        size = lines // 2
+        view = w_planes.at[owner, part * size : part * size + size]
+        return remote(view, view, o_send.at[slot], o_recv.at[slot], target)
+
+    def open_plane(make):
+        first = [
+            make(spot, 0, 0, beside_peer),
+            make(spot, 1, 2, across_peer),
+            make(spot, 1, 1, beside_peer),
+            make(spot, 0, 3, across_peer),
+        ]
+        for copy in first:
+            copy.start()
+        return first
+
+    def relay_plane(make, first):
+        first[0].wait_recv()
+        ahead = make(beside, 0, 4, across_peer)
+        ahead.start()
+        first[1].wait_recv()
+        aside = make(across, 1, 5, beside_peer)
+        aside.start()
+        return [ahead, aside]
+
+    def close_plane(first, second):
+        first[2].wait_recv()
+        first[3].wait_recv()
+        for copy in first:
+            copy.wait_send()
+        for copy in second:
+            copy.wait()
+
+    w_first = open_plane(w_copy)
+    x_copies, z_copies, p_copies = [], [], []
     for step in range(1, lines):
         other, target = line_peer(step)
         copy = remote(
@@ -121,34 +179,18 @@
         copy.start()
         x_copies.append(copy)
     for step in range(1, lines):
-        copy = remote(
-            w_out_ref,
-            w_all_ref.at[spot, line],
-            z_send.at[step],
-            z_recv.at[step],
-            line_peer(step)[1],
-        )
+        own = w_planes.at[spot, line]
+        copy = remote(own, own, z_send.at[step], z_recv.at[step], line_peer(step)[1])
         copy.start()
         z_copies.append(copy)
     spread[line] = normed[:, pl.ds(pl.multiple_of(line * block, block), block)]
-    keep_out.wait()
+    w_second = relay_plane(w_copy, w_first)
+    for copy in z_copies:
+        copy.wait()
+    o_first = open_plane(o_copy)
     for copy in x_copies:
         copy.wait()
-    for copy in z_copies:
-        copy.wait()
-    for step in range(1, PLANE):
-        copy = remote(
-            w_all_ref.at[spot],
-            w_all_ref.at[spot],
-            o_send.at[step],
-            o_recv.at[step],
-            plane_peer(step),
-        )
-        copy.start()
-        o_copies.append(copy)
-    for copy in w_copies:
-        copy.wait()
-    main = weights.shape[1] - LANES
+    close_plane(w_first, w_second)
     product = jnp.dot(
         spread[...].reshape(lines * rows, block),
         weights[...],
@@ -170,28 +212,186 @@
         )
         copy.start()
         p_copies.append(copy)
+    o_second = relay_plane(o_copy, o_first)
     total = partial[line]
     for step in range(1, lines):
         p_copies[step - 1].wait()
         total = total + arrived[step].astype(jnp.float32)
     proj_ref[...] = total
-    for copy in o_copies:
+    close_plane(o_first, o_second)
+    store = pltpu.make_async_copy(w_planes, w_all_ref, local_sem.at[0])
+    store.start()
+    store.wait()
+
+
+def cell_kernel(
+    proj_ref,
+    ibias_hbm,
+    fbias_hbm,
+    head_gain_hbm,
+    matrix_hbm,
+    norm_hbm,
+    max_hbm,
+    cell_ref,
+    new_matrix_ref,
+    new_norm_ref,
+    new_max_ref,
+    ibias_ref,
+    fbias_ref,
+    head_gain_ref,
+    matrix,
+    state_norm,
+    state_max,
+    turned,
+    decay,
+    left,
+    keys,
+    queries,
+    reads,
+    sems,
+    in_sems,
+    out_sems,
+):
+    rows, heads, size, _ = matrix.shape
+    wide = heads * size
+    pack = 2 * heads
+    chunk = 8
+    chunks = rows // chunk
+    loads = []
+    for index in range(chunks):
+        part = pl.ds(index * chunk, chunk)
+        copy = pltpu.make_async_copy(matrix_hbm.at[part], matrix.at[part], in_sems.at[index])
+        copy.start()
+        loads.append(copy)
+    small = fetch_all(
+        (
+            (ibias_hbm, ibias_ref),
+            (fbias_hbm, fbias_ref),
+            (head_gain_hbm, head_gain_ref),
+            (norm_hbm, state_norm),
+            (max_hbm, state_max),
+        ),
+        sems,
+    )
+    turned[...] = jnp.zeros_like(turned)
+    gates = proj_ref[:, 4 * wide :]
+    gates = gates + pltpu.roll(gates, LANES // 2, 1)
+    forget = pltpu.roll(gates, LANES - heads, 1)
+    for copy in small:
+        copy.wait()
+    turned[:heads, :rows] = state_max[...]
+    old_max = turned[...].T[:rows]
+    turned[...] = jnp.zeros_like(turned)
+    turned[0:1, :heads] = ibias_ref[...]
+    turned[1:2, :heads] = fbias_ref[...]
+    input_pre = gates + turned[0:1, :]
+    forget_pre = forget + turned[1:2, :]
+    log_forget = jnp.minimum(forget_pre, 0.0) - jnp.log(1.0 + jnp.exp(-jnp.abs(forget_pre)))
+    new_max = jnp.maximum(log_forget + old_max, input_pre)
+    keep_old = jnp.exp(log_forget + old_max - new_max)
+    keep_new = jnp.exp(input_pre - new_max)
+    turned[:rows, :] = new_max
+    new_max_ref[...] = turned[...].T[:heads, :rows]
+    place = lax.broadcasted_iota(jnp.int32, (rows, pack, LANES), 1)
+    lane = lax.broadcasted_iota(jnp.int32, (rows, pack, LANES), 2)
+    chosen = (place == lane) | (place == lane + heads)
+
+    def per_head(values):
+        spread = jnp.broadcast_to(values[:, None, :], (rows, pack, LANES))
+        return jnp.sum(
+            jnp.where(chosen & (lane < heads), spread, 0.0), axis=-1, keepdims=True
+        )
+
+    old_scale = per_head(keep_old)
+    new_scale = per_head(keep_new)
+    floor = per_head(jnp.exp(-new_max))
+    decay[...] = jnp.broadcast_to(old_scale, decay.shape)
+    row = lax.broadcasted_iota(jnp.int32, (rows, pack, wide), 1)
+    head = lax.broadcasted_iota(jnp.int32, (rows, pack, wide), 2) // size
+    same = (row == head) | (row == head + heads)
+    fold = (
+        lax.broadcasted_iota(jnp.int32, (wide, size), 0) % size
+        == lax.broadcasted_iota(jnp.int32, (wide, size), 1)
+    ).astype(jnp.float32).astype(jnp.bfloat16)
+
+    def rounded(index):
+        return proj_ref[:, index * wide : (index + 1) * wide].astype(jnp.bfloat16).astype(jnp.float32)
+
+    def split_heads(values):
+        spread = jnp.broadcast_to(values[:, None, :], (rows, pack, wide))
+        masked = jnp.where(same, spread, 0.0).reshape(rows * pack, wide).astype(jnp.bfloat16)
+        return jnp.dot(masked, fold, preferred_element_type=jnp.float32).reshape(
+            rows, pack, size
+        )
+
+    query = split_heads(rounded(0))
+    key = split_heads(rounded(1)) * size ** (-0.5)
+    value = jnp.broadcast_to(rounded(2)[:, None, :], (rows, pack, wide))
+    value = jnp.where(same, value * new_scale, 0.0)
+    coarse = value.astype(jnp.bfloat16).astype(jnp.float32)
+    left[...] = jnp.where(row < heads, coarse, value - coarse)
+    keys[...] = key
+    queries[...] = query
+    new_norm = old_scale[:, :heads] * state_norm[...] + (new_scale * key)[:, :heads]
+    new_norm_ref[...] = new_norm
+    divisor = jnp.sum(new_norm * query[:, :heads], axis=-1, keepdims=True)
+    divisor = jnp.maximum(jnp.abs(divisor), floor[:, :heads])
+    stores = []
+    for index in range(chunks):
+        loads[index].wait()
+
+        @pl.loop(0, chunk // 4)
+        def _(group):
+            for inner in range(4):
+                item = index * chunk + group * 4 + inner
+                outer = lax.dot_general(
+                    left[item].astype(jnp.bfloat16),
+                    keys[item].astype(jnp.bfloat16),
+                    (((0,), (0,)), ((), ())),
+                    preferred_element_type=jnp.float32,
+                ).reshape(heads, size, size)
+                scale = decay[item][:heads][:, None, :]
+                fresh = scale * matrix[item] + outer
+                matrix[item] = fresh
+                flat = fresh.reshape(wide, size)
+                high = flat.astype(jnp.bfloat16)
+                low = (flat - high.astype(jnp.float32)).astype(jnp.bfloat16)
+                asked = queries[item].astype(jnp.bfloat16)
+                reads[item] = dot_t(asked, high) + dot_t(asked, low)
+
+        part = pl.ds(index * chunk, chunk)
+        copy = pltpu.make_async_copy(matrix.at[part], new_matrix_ref.at[part], out_sems.at[index])
+        copy.start()
+        stores.append(copy)
+    only = (row == head)[:, :heads]
+    read = jnp.where(only, reads[:, :heads, :] / divisor, 0.0)
+    mean = jnp.sum(read, axis=-1, keepdims=True) / size
+    centered = jnp.where(only, read - mean, 0.0)
+    variance = jnp.sum(centered * centered, axis=-1, keepdims=True) / size
+    scaled = jnp.sum(centered * lax.rsqrt(variance + 1e-06), axis=1)
+    cell_ref[...] = (scaled * head_gain_ref[...] * jax.nn.sigmoid(rounded(3))).astype(jnp.bfloat16)
+    for copy in stores:
         copy.wait()
 
 
 def expert_kernel(
     count,
+    cell_hbm,
+    w_all_hbm,
+    tokens_hbm,
+    gain_hbm,
+    routes_hbm,
+    route_weights_hbm,
+    w_gate_hbm,
+    w_up_hbm,
+    w_down_hbm,
+    mixed_ref,
     cell_ref,
     w_all_ref,
     tokens_ref,
     gain_ref,
-    target_rows_ref,
-    target_cols_ref,
+    routes_ref,
     route_weights_ref,
-    w_gate_hbm,
-    w_up_hbm,
-    w_down_hbm,
-    mixed_ref,
     w_gate,
     w_up,
     w_down,
@@ -222,20 +422,30 @@
     rows, width = tokens_ref.shape
     half = width // 2
     slots = count * SLOT_TILE
-    top = route_weights_ref.shape[1]
-    loads = []
-    for index, (source, kept) in enumerate(
-        ((w_gate_hbm, w_gate), (w_up_hbm, w_up), (w_down_hbm, w_down))
-    ):
-        copy = pltpu.make_async_copy(source, kept, local_sem.at[index])
-        copy.start()
-        loads.append(copy)
+    top = route_weights_ref.shape[0]
+    loads = fetch_all(
+        (
+            (cell_hbm, cell_ref),
+            (w_all_hbm, w_all_ref),
+            (tokens_hbm, tokens_ref),
+            (gain_hbm, gain_ref),
+            (routes_hbm, routes_ref),
+            (route_weights_hbm, route_weights_ref),
+            (w_gate_hbm, w_gate),
+            (w_up_hbm, w_up),
+            (w_down_hbm, w_down),
+        ),
+        local_sem,
+    )
     barrier = pltpu.get_barrier_semaphore()
     for step in range(1, count):
         pl.semaphore_signal(
             barrier, inc=1, device_id=(lax.rem(ep + step, count), tp), device_id_type=MESH
         )
     pl.semaphore_signal(barrier, inc=1, device_id=partner, device_id_type=MESH)
+    for copy in loads[:6]:
+        copy.wait()
+    loads = loads[6:]
     cell = cell_ref[...]
     columns = w_all_ref.shape[3]
     lines = w_all_ref.shape[1]
@@ -248,11 +458,27 @@
     pl.semaphore_wait(barrier, count)
     swap = remote(mine, theirs, t_send.at[0], t_recv.at[0], partner)
     swap.start()
-    slot_row = lax.broadcasted_iota(jnp.int32, (slots, rows), 0)
+    slot_row = lax.broadcasted_iota(jnp.int32, (slots, rows), 0).astype(jnp.float32)
+    expert = lax.broadcasted_iota(jnp.int32, (count, rows), 0).astype(jnp.float32)
+    before = (
+        lax.broadcasted_iota(jnp.int32, (rows, rows), 0)
+        < lax.broadcasted_iota(jnp.int32, (rows, rows), 1)
+    ).astype(jnp.float32)
+    taken = jnp.zeros((count, 1), jnp.float32)
     dispatch = jnp.zeros((slots, rows), jnp.float32)
+    combine = jnp.zeros((slots, rows), jnp.float32)
     for k in range(top):
-        dispatch += jnp.where(slot_row == target_rows_ref[k : k + 1, :], 1.0, 0.0)
+        named = routes_ref[k : k + 1, :].astype(jnp.float32)
+        match = jnp.where(expert == named, 1.0, 0.0)
+        earlier = jnp.dot(match, before, preferred_element_type=jnp.float32) + taken
+        taken = taken + jnp.sum(match, axis=1, keepdims=True)
+        target = named * SLOT_TILE + jnp.sum(match * earlier, axis=0, keepdims=True)
+        hit = slot_row == target
+        dispatch += jnp.where(hit, 1.0, 0.0)
+        combine += jnp.where(hit, route_weights_ref[k : k + 1, :], 0.0)
     dispatch = dispatch.astype(jnp.bfloat16)
+    coarse = combine.astype(jnp.bfloat16)
+    fine = (combine - coarse.astype(jnp.float32)).astype(jnp.bfloat16)
     swap.wait()
     summed = mine[...].astype(jnp.float32) + theirs[...].astype(jnp.float32)
     resid[...] = (tokens_ref[...].astype(jnp.float32) + summed).astype(jnp.bfloat16)
@@ -325,20 +551,13 @@
         copy.start()
         sends.append(copy)
     returned[ep] = finished[ep]
-    slot_col = lax.broadcasted_iota(jnp.int32, (rows, slots), 1)
-    combine = jnp.zeros((rows, slots), jnp.float32)
-    for k in range(top):
-        combine += jnp.where(
-            slot_col == target_cols_ref[:, k : k + 1], route_weights_ref[:, k : k + 1], 0.0
-        )
-    coarse = combine.astype(jnp.bfloat16)
-    fine = (combine - coarse.astype(jnp.float32)).astype(jnp.bfloat16)
     for copy in sends:
         copy.wait()
     back = returned[...].reshape(slots, half)
-    weighted = jnp.dot(coarse, back, preferred_element_type=jnp.float32) + jnp.dot(
-        fine, back, preferred_element_type=jnp.float32
-    )
+    turn = (((0,), (0,)), ((), ()))
+    weighted = lax.dot_general(
+        coarse, back, turn, preferred_element_type=jnp.float32
+    ) + lax.dot_general(fine, back, turn, preferred_element_type=jnp.float32)
     last_send[...] = (resid[:, my_half].astype(jnp.float32) + weighted).astype(jnp.bfloat16)
     swap = remote(last_send, last_recv, t_send.at[2], t_recv.at[2], partner)
     swap.start()
@@ -353,54 +572,106 @@
     depth, columns = w_query.shape
     lines = lax.axis_size("ep") // PLANE
     heads = w_igate.shape[1]
-    pair = jnp.concatenate((w_igate, w_fgate), axis=1)
-    pad = jnp.zeros((depth, LANES // 2 - 2 * heads), pair.dtype)
-    gates = jnp.concatenate((pair, pad, pair, pad), axis=1)
     total = 4 * columns + LANES
     vmem = pl.BlockSpec(memory_space=pltpu.VMEM)
     anywhere = pl.BlockSpec(memory_space=pl.ANY)
     dma = pltpu.SemaphoreType.DMA
-    proj, w_all = pl.pallas_call(
+    bf = jnp.bfloat16
+    planes = (PLANE, lines) + w_out.shape
+    return pl.pallas_call(
         functools.partial(mixer_kernel, lines),
         out_shape=(
             jax.ShapeDtypeStruct((rows, total), jnp.float32),
-            jax.ShapeDtypeStruct((PLANE, lines) + w_out.shape, jnp.bfloat16),
+            jax.ShapeDtypeStruct(planes, bf),
         ),
-        in_specs=[vmem, vmem] + [anywhere] * 5 + [vmem],
+        in_specs=[anywhere] * 9,
         out_specs=(vmem, anywhere),
         scratch_shapes=[
-            pltpu.VMEM((rows, width), jnp.bfloat16),
-            pltpu.VMEM((lines, rows, depth * PLANE), jnp.bfloat16),
-            pltpu.VMEM((depth * PLANE, total), jnp.bfloat16),
+            pltpu.VMEM((rows, width), bf),
+            pltpu.VMEM((1, width), jnp.float32),
+            pltpu.VMEM((heads, depth), bf),
+            pltpu.VMEM((heads, depth), bf),
+            pltpu.VMEM((LANES, depth), jnp.float32),
+            pltpu.VMEM(planes, bf),
+            pltpu.VMEM((rows, width), bf),
+            pltpu.VMEM((lines, rows, depth * PLANE), bf),
+            pltpu.VMEM((depth * PLANE, total), bf),
             pltpu.VMEM((lines, rows, total), jnp.float32),
-            pltpu.VMEM((lines, rows, total), jnp.bfloat16),
-            pltpu.VMEM((lines, rows, total), jnp.bfloat16),
+            pltpu.VMEM((lines, rows, total), bf),
+            pltpu.VMEM((lines, rows, total), bf),
+            dma((9,)),
             dma((6,)),
-            dma((PLANE,)),
-            dma((PLANE,)),
+            dma((6,)),
             dma((lines,)),
             dma((lines,)),
             dma((lines,)),
             dma((lines,)),
             dma((lines,)),
             dma((lines,)),
-            dma((PLANE,)),
-            dma((PLANE,)),
+            dma((6,)),
+            dma((6,)),
         ],
         compiler_params=pltpu.CompilerParams(
-            collective_id=0, has_side_effects=True, vmem_limit_bytes=16 * 1024 * 1024
+            collective_id=0, has_side_effects=True, vmem_limit_bytes=VMEM_BYTES
         ),
-    )(tokens, mix_gain[None, :], w_query, w_key, w_value, w_outgate, gates, w_out)
-    main = 4 * columns
-    gate_sums = proj[:, main : main + LANES // 2] + proj[:, main + LANES // 2 :]
-    return (
-        proj[:, :columns],
-        proj[:, columns : 2 * columns],
-        proj[:, 2 * columns : 3 * columns],
-        proj[:, 3 * columns : main],
-        gate_sums[:, :heads],
-        gate_sums[:, heads : 2 * heads],
-    ), w_all
+    )(
+        tokens,
+        mix_gain[None, :],
+        w_query,
+        w_key,
+        w_value,
+        w_outgate,
+        jnp.swapaxes(w_igate, 0, 1),
+        jnp.swapaxes(w_fgate, 0, 1),
+        w_out,
+    )
+
+
+def cell_call(proj, igate_bias, fgate_bias, head_gain, state_matrix, state_norm, state_max):
+    rows, heads, size, _ = state_matrix.shape
+    wide = heads * size
+    vmem = pl.BlockSpec(memory_space=pltpu.VMEM)
+    anywhere = pl.BlockSpec(memory_space=pl.ANY)
+    dma = pltpu.SemaphoreType.DMA
+    f32 = jnp.float32
+    cell_out, new_matrix, new_norm, new_max = pl.pallas_call(
+        cell_kernel,
+        out_shape=(
+            jax.ShapeDtypeStruct((rows, wide), jnp.bfloat16),
+            jax.ShapeDtypeStruct(state_matrix.shape, f32),
+            jax.ShapeDtypeStruct(state_norm.shape, f32),
+            jax.ShapeDtypeStruct((heads, rows), f32),
+        ),
+        in_specs=[vmem] + [anywhere] * 6,
+        out_specs=(vmem, anywhere, vmem, vmem),
+        scratch_shapes=[
+            pltpu.VMEM((1, heads), f32),
+            pltpu.VMEM((1, heads), f32),
+            pltpu.VMEM((1, wide), f32),
+            pltpu.VMEM(state_matrix.shape, f32),
+            pltpu.VMEM(state_norm.shape, f32),
+            pltpu.VMEM((heads, rows), f32),
+            pltpu.VMEM((LANES, LANES), f32),
+            pltpu.VMEM((rows, 2 * heads, size), f32),
+            pltpu.VMEM((rows, 2 * heads, wide), f32),
+            pltpu.VMEM((rows, 2 * heads, size), f32),
+            pltpu.VMEM((rows, 2 * heads, size), f32),
+            pltpu.VMEM((rows, 2 * heads, wide), f32),
+            dma((5,)),
+            dma((rows // 8,)),
+            dma((rows // 8,)),
+        ],
+        compiler_params=pltpu.CompilerParams(vmem_limit_bytes=VMEM_BYTES),
+    )(
+        proj,
+        igate_bias[None, :],
+        fgate_bias[None, :],
+        head_gain[None, :],
+        state_matrix,
+        state_norm,
+        jnp.swapaxes(state_max, 0, 1),
+    )
+    return cell_out, new_matrix, new_norm, jnp.swapaxes(new_max, 0, 1)
 
 
 def expert_call(
@@ -408,12 +679,6 @@
 ):
     rows, width = tokens.shape
     count = lax.axis_size("ep")
-    flat = routes.reshape(-1)
-    same = (flat[:, None] == flat[None, :]).astype(jnp.int32)
-    order = jnp.arange(flat.shape[0], dtype=jnp.int32)
-    earlier = (order[None, :] < order[:, None]).astype(jnp.int32)
-    slots = jnp.sum(same * earlier, axis=1, dtype=jnp.int32)
-    targets = (flat * SLOT_TILE + slots).reshape(routes.shape)
     gate_t = jnp.swapaxes(w_gate[0], 0, 1)
     up_t = jnp.swapaxes(w_up[0], 0, 1)
     down = w_down[0]
@@ -427,9 +692,15 @@
     return pl.pallas_call(
         functools.partial(expert_kernel, count),
         out_shape=jax.ShapeDtypeStruct((rows, width), bf),
-        in_specs=[vmem] * 7 + [anywhere] * 3,
+        in_specs=[anywhere] * 9,
         out_specs=vmem,
         scratch_shapes=[
+            pltpu.VMEM(cell_out.shape, bf),
+            pltpu.VMEM(w_all.shape, bf),
+            pltpu.VMEM((rows, width), bf),
+            pltpu.VMEM((1, width), jnp.float32),
+            pltpu.VMEM((routes.shape[1], rows), jnp.int32),
+            pltpu.VMEM((routes.shape[1], rows), jnp.float32),
             pltpu.VMEM(gate_t.shape, bf),
             pltpu.VMEM(up_t.shape, bf),
             pltpu.VMEM(down.shape, bf),
@@ -445,7 +716,7 @@
             pltpu.VMEM(tile, bf),
             pltpu.VMEM((rows, half), bf),
             pltpu.VMEM((rows, half), bf),
-            dma((3,)),
+            dma((9,)),
             dma((3,)),
             dma((3,)),
             dma((count,)),
@@ -456,16 +727,15 @@
             dma((count,)),
         ],
         compiler_params=pltpu.CompilerParams(
-            collective_id=1, has_side_effects=True, vmem_limit_bytes=40 * 1024 * 1024
+            collective_id=1, has_side_effects=True, vmem_limit_bytes=VMEM_BYTES
         ),
     )(
         cell_out,
         w_all,
         tokens,
         ffn_gain[None, :],
-        jnp.swapaxes(targets, 0, 1),
-        targets,
-        route_weights,
+        jnp.swapaxes(routes, 0, 1),
+        jnp.swapaxes(route_weights, 0, 1),
         gate_t,
         up_t,
         down,
@@ -527,13 +797,14 @@
     capacity = max(2, 2 * rows * routes.shape[1] // (w_expert_gate.shape[0] * ep_count))
     return (
         lax.axis_size("tp") == 2
-        and ep_count % PLANE == 0
-        and w_query.shape[0] % LANES == 0
+        and ep_count % (2 * PLANE) == 0
+        and w_query.shape[0] == LANES
         and w_query.shape[1] % LANES == 0
         and w_out.shape[1] % LANES == 0
         and width % (2 * LANES) == 0
         and rows % SLOT_TILE == 0
-        and w_igate.shape[1] * 4 <= LANES
+        and w_igate.shape[1] == 4
+        and rows <= LANES
         and w_expert_gate.shape[0] == 1
         and capacity <= SLOT_TILE
     )
@@ -565,18 +836,9 @@
     seq_rows, width = tokens.shape
     weight_list = (w_query, w_key, w_value, w_outgate, w_igate, w_fgate)
     if kernels_fit(tokens, w_query, w_igate, w_out, w_expert_gate, routes):
-        projected, w_all = mixer_call(tokens, mix_gain, weight_list, w_out)
-        cell_out, new_matrix, new_norm, new_max = memory_cell(
-            projected[0].astype(jnp.bfloat16),
-            projected[1].astype(jnp.bfloat16),
-            projected[2].astype(jnp.bfloat16),
-            projected[3].astype(jnp.bfloat16),
-            projected[4] + igate_bias,
-            projected[5] + fgate_bias,
-            head_gain,
-            state_matrix,
-            state_norm,
-            state_max,
+        proj, w_all = mixer_call(tokens, mix_gain, weight_list, w_out)
+        cell_out, new_matrix, new_norm, new_max = cell_call(
+            proj, igate_bias, fgate_bias, head_gain, state_matrix, state_norm, state_max
         )
         mixed = expert_call(
             cell_out,

time: 102 us -> 76.7 us (0.75)
  local copies, waits for them, and re-layouts: 16.5 us -> 1.57 us
  other arithmetic: 9.86 us -> 0 us
  matrix products: 5.7 us -> 0 us
  Pallas kernels: 68.7 us -> 74.2 us
    unnamed x41 -> x1, local copies, waits for them, and re-layouts: 15.5 us -> 1.57 us
    pallas_call x0 -> x1, Pallas kernels: none -> 9.89 us  [cell_call(): pl.pallas_call(cell_kernel, out_shape=(jax.ShapeDtypeStruct((rows, wide),...]
    add x3 -> x0, other arithmetic: 5.96 us -> none  [the longest x1 5.88 us: memory_cell(): keep_old[:, :, None, None] * state_matrix]
    pallas_call x1, Pallas kernels: 28 us -> 22.1 us  [mixer_call(): pl.pallas_call(functools.partial(mixer_kernel, lines), out_shape=(jax.Sha...]
    dot_general x1 -> x0, matrix products: 5.7 us -> none  [memory_cell(): jnp.einsum('bhvd,bhd->bhv', new_matrix, query_heads, precision=lax.Precis...]
    reduce_sum x4 -> x0, other arithmetic: 2.17 us -> none  [the longest x1 1.63 us: memory_cell(): denominator = jnp.sum(new_norm * query_heads, axis=-1)]
    pallas_call x1, Pallas kernels: 40.7 us -> 42.2 us  [expert_call(): pl.pallas_call(functools.partial(expert_kernel, count), out_shape=jax.Sha...]
where the time goes in v2:
time: 76.7 us; the launch traced here: 76.4 us
  Pallas kernels  74.2 us (97%)
  local copies, waits for them, and re-layouts  1.57 us (2%)
    pallas_call x1, Pallas kernels, expert_call(): pl.pallas_call(functools.partial(expert_kernel, count), out_shape=jax.Sha...  42.2 us
    pallas_call x1, Pallas kernels, mixer_call(): pl.pallas_call(functools.partial(mixer_kernel, lines), out_shape=(jax.Sha...  22.1 us
    pallas_call x1, Pallas kernels, cell_call(): pl.pallas_call(cell_kernel, out_shape=(jax.ShapeDtypeStruct((rows, wide),...  9.89 us
    unnamed x1, local copies, waits for them, and re-layouts  1.57 us

profile of v2, /device:TPU:29, one launch (start us, length us, event | category | flops | bytes accessed | tf_op | source)
XLA Modules:
  0.0 76.4 jit_solution(11527869408130246485)
XLA Ops:
  0.6 22.1 %shard_map.228 = (f32[32,1152]{1,0:T(8,128)}, bf16[4,4,256,128]{3,2,1,0:T(8,128)(2,1)}) custom-call(bf16[32,2048]{1,0:T(8,128)(2,1)} %tokens_hbm.3, f32[1,2048]{1,0:T(1,128)} %bitcast.21, bf16[128,256]{1,0:T(8,128)(2,1)} %wq_ref.1, bf16[128,256]{1,0:T(8,128)(2,1)} %wk_ref.1, bf16[128,256]{1,0:T(8,128)(2,1)} %wv_ref.1, bf16[128,256]{1,0:T(8,128)(2,1)} %wo_gate_ref.1, ...), custom_call_target="tpu_custom_call" | custom-call | tf_op jit(solution)/shard_map/pallas_call | solution.py:581
  22.7 9.9 %shard_map.229 = (bf16[32,256]{1,0:T(8,128)(2,1)}, f32[32,4,64,64]{3,2,1,0:T(8,128)}, f32[32,4,64]{2,1,0:T(4,128)}, f32[4,32]{1,0:T(4,128)}) custom-call(f32[32,1152]{1,0:T(8,128)} %get-tuple-element.10.proj_ref, f32[1,4]{1,0:T(1,128)} %bitcast.29, f32[1,4]{1,0:T(1,128)} %bitcast.30, f32[1,256]{1,0:T(1,128)} %bitcast.28, f32[32,4,64,64]{3,2,1,0:T(8,128)} %matrix_hbm.1, ...), custom_call_target="tpu_custom_call" | custom-call | tf_op jit(solution)/shard_map/pallas_call | solution.py:637
  32.6 42.2 %shard_map.230 = bf16[32,2048]{1,0:T(8,128)(2,1)} custom-call(bf16[32,256]{1,0:T(8,128)(2,1)} %get-tuple-element.11.cell_hbm, bf16[4,4,256,128]{3,2,1,0:T(8,128)(2,1)} %get-tuple-element.12.w_all_hbm, bf16[32,2048]{1,0:T(8,128)(2,1)} %tokens_hbm.3, f32[1,2048]{1,0:T(1,128)} %bitcast.22, s32[3,32]{1,0:T(4,128)} %bitcast.24, f32[3,32]{1,0:T(4,128)} %bitcast.25, ...), custom_call_target="tpu_custom_call" | custom-call | tf_op jit(solution)/shard_map/pallas_call | solution.py:692
  74.9 1.6 %copy.26 = bf16[32,2048]{1,0:T(8,128)(2,1)} copy(bf16[32,2048]{1,0:T(8,128)(2,1)} %shard_map.230) | data formatting | bytes 262144
